TPU v7x, 256 devices: a whole 4x4x8 slice. The times are simulated.
256 devices in a mesh: ep: 64 (over z, x, core), tp: 4 (over y).
Axes of the slice: x: 4, y: 4, z: 8, core: 2. Of those that a mesh axis runs over, the one named last changes fastest.
Arguments:
- pool_in: bfloat16 [65536, 1024], P(('ep', 'tp')), may hold values from -6 to 6
- w_pool: bfloat16 [8, 128, 128], replicated, may hold values from -0.5 to 0.5
- pool_scale: float32 [1024], replicated, may hold values from 0.1 to 1.9
- w_out: bfloat16 [1024, 2048], replicated, may hold values from -0.1875 to 0.1875
- expert_in: bfloat16 [32768, 2048], P('ep'), may hold values from -6 to 6
- ffn_gain: float32 [2048], replicated, may hold values from 0.1 to 1.9
- routes: int32 [32768, 2], P('ep'), may hold values from 0 to 63, all different within a row; in each aligned block of 128 rows (0 to 127, 128 to 255, ...) at most 6 rows name the same one
- route_weight: float32 [32768, 2], P('ep'), may hold values from 0.25 to 1
- w_gate: bfloat16 [64, 2048, 1024], P('ep', None, 'tp'), may hold values from -0.125 to 0.125
- w_up: bfloat16 [64, 2048, 1024], P('ep', None, 'tp'), may hold values from -0.125 to 0.125
- w_down: bfloat16 [64, 1024, 2048], P('ep', 'tp'), may hold values from -0.1875 to 0.1875
Outputs:
- mixer_out: bfloat16 [65536, 2048], P(('ep', 'tp'))
- expert_out: bfloat16 [32768, 2048], P(('ep', 'tp'))
Inputs may be any that keep to these rules, and one draw needn't show every extreme that they name: `routes`: each row names 2 different experts. In each aligned block of 128 rows no expert is named by more than 6 rows, and in some block some expert is named by exactly 6 rows.
All inputs are finite; a program needn't handle non-finite values.
Results may differ from a plain program's by a relative error of at most 0.012.
Values may be sent and summed in bfloat16 or wider, within the bound.
No kernel may reach another device: no remote copies, remote signals or barrier semaphores. Data moves between devices by JAX's collectives and lax.ppermute only.
A program may use at most 128 MiB of HBM per device.

v0:
```python
from functools import partial
import jax
import jax.numpy as jnp
from jax import lax
from jax.sharding import PartitionSpec as P

GDIM = 128
WMAX = 16
K = 2
EPS = 0.05


def passed_along(array, axis, by):
    length = lax.axis_size(axis)
    pairs = [(i, i + by) for i in range(length) if 0 <= i + by < length]
    return lax.ppermute(array, axis, pairs)


def rows_first(arrays, axis, dims):
    turned = [jnp.moveaxis(a, dim, 0) for a, dim in zip(arrays, dims)]
    both = jnp.concatenate([t.reshape(len(t), -1) for t in turned], axis=1)
    out, at, gathered = (lax.all_gather(both, axis, axis=0, tiled=True), 0, [])
    for t, dim in zip(turned, dims):
        piece = out[:, at : at + t[0].size].reshape(-1, *t.shape[1:])
        gathered.append(jnp.moveaxis(piece, 0, dim))
        at += t[0].size
    return tuple(gathered)


def window_sizes(width):
    group_of = jnp.arange(width) // GDIM
    level = group_of % 4
    return jnp.where(
        level == 0, 2.0, jnp.where(level == 1, 4.0, jnp.where(level == 2, 8.0, 16.0))
    ).astype(jnp.float32)


def pooled_rows(extended, positions):
    extent = extended.shape[0] - (WMAX - 1)
    window = window_sizes(extended.shape[1])
    running = jnp.zeros((extent, extended.shape[1]), jnp.float32)
    picked = running
    for offset in range(WMAX):
        running = running + extended[WMAX - 1 - offset : WMAX - 1 - offset + extent]
        if offset + 1 in (2, 4, 8, 16):
            picked = jnp.where(window[None, :] == offset + 1, running, picked)
    counted = jnp.minimum(positions[:, None] + 1.0, window[None, :])
    return (picked / counted - extended[WMAX - 1 :]).astype(jnp.bfloat16)


def normalize(features_in, gain):
    features = features_in.astype(jnp.float32)
    inverse = lax.rsqrt(jnp.mean(features * features, axis=-1, keepdims=True) + EPS)
    return (features * inverse * gain).astype(jnp.bfloat16)


def slot_places(expert_ids, experts, capacity):
    onehot = (expert_ids[:, None] == jnp.arange(experts)[None, :]).astype(jnp.int32)
    earlier = jnp.cumsum(onehot, axis=0) - onehot
    slot_rank = jnp.sum(earlier * onehot, axis=1)
    return expert_ids * capacity + slot_rank


def send_block(normed_block, places, experts, capacity):
    pairs = places.shape[0]
    table = (
        jnp.full((experts * capacity,), pairs, jnp.int32)
        .at[places]
        .set(jnp.arange(pairs, dtype=jnp.int32))
    )
    source = jnp.where(table < pairs, table // K, normed_block.shape[0])
    padded = jnp.concatenate(
        [normed_block, jnp.zeros((1, normed_block.shape[1]), normed_block.dtype)], axis=0
    )
    return padded[source].reshape(experts, capacity, normed_block.shape[1])


def on_device(
    pool_in,
    w_pool,
    pool_scale,
    w_out,
    expert_in,
    ffn_gain,
    routes,
    route_weight,
    w_gate,
    w_up,
    w_down,
):
    rows_here = pool_in.shape[0]
    before = passed_along(pool_in[rows_here - (WMAX - 1) :], ("ep", "tp"), 1)
    extended = jnp.concatenate([before, pool_in], axis=0).astype(jnp.float32)
    positions = (lax.axis_index(("ep", "tp")) * rows_here + jnp.arange(rows_here)).astype(
        jnp.float32
    )
    pooled = pooled_rows(extended, positions)
    group_count = w_pool.shape[0]
    grouped = jnp.einsum(
        "tgc,gcd->tgd",
        pooled.reshape(rows_here, group_count, GDIM),
        w_pool,
        preferred_element_type=jnp.float32,
    )
    scaled = (grouped.reshape(rows_here, -1) * pool_scale).astype(jnp.bfloat16)
    mixer_out = jnp.dot(scaled, w_out, preferred_element_type=jnp.float32).astype(jnp.bfloat16)
    parts = lax.axis_size("tp")
    own = lax.axis_index("tp")
    experts = lax.axis_size("ep") * w_gate.shape[0]
    block_rows = routes.shape[0] // parts
    capacity = 3 * block_rows * K // (2 * experts)
    width = expert_in.shape[1]
    route_blocks = routes.reshape(parts, block_rows * K)
    weight_blocks = route_weight.reshape(parts, block_rows * K)
    places = jax.vmap(partial(slot_places, experts=experts, capacity=capacity))(route_blocks)
    gate_local = w_gate[0]
    up_local = w_up[0]
    down_local = w_down[0]
    gate_whole, up_whole, down_whole = rows_first(
        (gate_local, up_local, down_local), "tp", (1, 1, 0)
    )
    mine = lax.dynamic_slice_in_dim(expert_in, own * block_rows, block_rows, 0)
    own_places = lax.dynamic_index_in_dim(places, own, 0, keepdims=False)
    outgoing = send_block(normalize(mine, ffn_gain), own_places, experts, capacity)[None]
    arrived = lax.all_to_all(outgoing, "ep", split_axis=1, concat_axis=1, tiled=True)
    slot_rows = arrived.reshape(-1, width)
    gate_val = jnp.dot(slot_rows, gate_whole, preferred_element_type=jnp.float32)
    up_val = jnp.dot(slot_rows, up_whole, preferred_element_type=jnp.float32)
    hidden = (jax.nn.silu(gate_val) * up_val).astype(jnp.bfloat16)
    quarter = down_local.shape[0]
    total = jnp.zeros((slot_rows.shape[0], width), jnp.float32)
    for block in range(parts):
        partial_val = jnp.dot(
            hidden[:, block * quarter : (block + 1) * quarter],
            down_whole[block * quarter : (block + 1) * quarter],
            preferred_element_type=jnp.float32,
        ).astype(jnp.bfloat16)
        partial_val = lax.optimization_barrier(partial_val)
        total = total + partial_val.astype(jnp.float32)
    results = total.astype(jnp.bfloat16).reshape(experts, capacity, width)
    returned = lax.all_to_all(results, "ep", split_axis=0, concat_axis=0, tiled=True)
    mine_places = lax.dynamic_index_in_dim(places, own, 0, keepdims=False)
    mine_weights = lax.dynamic_index_in_dim(weight_blocks, own, 0, keepdims=False)
    values = returned.reshape(experts * capacity, width)[mine_places]
    weighted = values.astype(jnp.float32) * mine_weights[:, None]
    expert_out = jnp.sum(weighted.reshape(block_rows, K, width), axis=1).astype(jnp.bfloat16)
    return (mixer_out, expert_out)


def solution(mesh):
    placed = (
        P(("ep", "tp"), None),
        P(),
        P(),
        P(),
        P("ep", None),
        P(),
        P("ep", None),
        P("ep", None),
        P("ep", None, "tp"),
        P("ep", None, "tp"),
        P("ep", "tp", None),
    )
    return jax.shard_map(
        on_device,
        mesh=mesh,
        in_specs=placed,
        out_specs=(P(("ep", "tp"), None), P(("ep", "tp"), None)),
        check_vma=False,
    )
```

profile of v0, /device:TPU:96, one launch (start us, length us, event | category | flops | bytes accessed | tf_op | source)
XLA Modules:
  0.0 234.7 jit_solution(8038040765326191246)
XLA Ops:
  7.2 1.6 copy.36
  8.8 0.6 copy.35
  9.5 2.8 %pad_maximum_fusion = bf16[256,6144]{1,0:T(8,128)(2,1)} fusion(bf16[256,2048]{1,0:T(8,128)(2,1)} %bitcast.58, bf16[256,2048]{1,0:T(8,128)(2,1)S(1)} %bitcast.56, bf16[256,2048]{1,0:T(8,128)(2,1)S(1)} %bitcast.57), kind=kLoop, calls=%fused_computation.7 | loop fusion | flops 9437184 | bytes 6291456 | tf_op jit(solution)/shard_map/concatenate | solution.py:21
  12.4 0.6 copy-done.5
  13.2 0.2 eq.158
  13.5 2.4 %reduce-window.6 = s32[4,64,2,128]{3,1,2,0:T(8,128)S(1)} reduce-window(s32[4,64,2,128]{3,1,2,0:T(8,128)S(1)} %fusion.25, s32[]{:T(128)} %constant.95.clone.1), window={size=1x1x1x128 pad=0_0x0_0x0_0x127_0}, to_apply=%region_1.2 | reduce-window | flops 8323072 | bytes 524292 | tf_op jit(solution)/shard_map/reduce-window
  16.2 0.2 fusion.6
  16.5 0.2 fusion.8
  16.9 1.4 scatter_custom_fusion
  18.3 3.1 %gather_fusion = bf16[384,2048]{1,0:T(8,128)(2,1)} fusion(bf16[129,2048]{1,0:T(8,128)(2,1)S(1)} %concatenate.10, s32[1024]{0:T(1024)S(1)} %pad_clamp_fusion.1), kind=kCustom, calls=%fused_computation | custom fusion | bytes 3147264 | tf_op jit(solution)/shard_map/gather | solution.py:75
  21.4 2.5 %broadcast_in_dim_reshape.4 = bf16[1,64,6,2048]{3,2,1,0:T(8,128)(2,1)S(1)} reshape(bf16[384,2048]{1,0:T(8,128)(2,1)} %gather_fusion) | data formatting | bytes 3145728 | tf_op jit(solution)/shard_map/broadcast_in_dim;reshape | solution.py:124
  23.9 60.0 %all_to_all.10 = bf16[1,64,6,2048]{3,2,0,1:T(8,128)(2,1)} all-to-all(bf16[1,64,6,2048]{3,2,0,1:T(8,128)(2,1)S(1)} %bitcast.55), channel_id=1, replica_groups=mesh['ep'=64,'tp'=4] {'ep'}, dimensions={1} | all-to-all | bytes 3145728 | tf_op jit(solution)/shard_map/all_to_all | solution.py:125
  84.0 2.6 %reshape.143 = bf16[384,2048]{1,0:T(8,128)(2,1)S(1)} reshape(bf16[1,64,6,2048]{3,2,0,1:T(8,128)(2,1)} %all_to_all.10) | data formatting | bytes 3145728 | tf_op jit(solution)/shard_map/reshape | solution.py:126
  86.6 48.9 %all-gather.2.cloned.1.call-done = bf16[1024,6144]{1,0:T(8,128)(2,1)} async-done(((bf16[256,6144]{1,0:T(8,128)(2,1)}), bf16[1024,6144]{1,0:T(8,128)(2,1)}) %all-gather.2.cloned.1.call-update) | async-done | bytes 12582928 | tf_op jit(solution)/shard_map/all_gather | solution.py:22
  135.5 4.0 %fusion.2 = f32[384,1024]{1,0:T(8,128)S(1)} fusion(bf16[384,2048]{1,0:T(8,128)(2,1)S(1)} %reshape.143, bf16[1024,6144]{1,0:T(8,128)(2,1)} %all-gather.2.cloned.1.call-done), kind=kOutput, calls=%fused_computation.5 | convolution fusion | flops 1610612736 | bytes 7340032 | tf_op jit(solution)/shard_map/dot_general | solution.py:127
  139.5 4.1 %multiply_convert_fusion = bf16[384,1024]{1,0:T(8,128)(2,1)S(1)} fusion(f32[384,1024]{1,0:T(8,128)S(1)} %fusion.2, bf16[384,2048]{1,0:T(8,128)(2,1)S(1)} %reshape.143, bf16[1024,6144]{1,0:T(8,128)(2,1)} %all-gather.2.cloned.1.call-done), kind=kOutput, calls=%fused_computation.15 | convolution fusion | flops 1612972032 | bytes 8126464 | tf_op jit(solution)/shard_map/dot_general | solution.py:128
  143.6 1.8 convolution_convert_fusion.3
  145.4 1.8 convolution_convert_fusion.2
  147.2 1.8 convolution_convert_fusion.1
  149.0 1.8 convolution_convert_fusion
  150.8 1.2 add_convert_fusion
  152.1 1.6 reshape.144
  153.6 10.6 %all-to-all-start.1 = ((bf16[64,6,2048]{2,1,0:T(8,128)(2,1)}), bf16[64,6,2048]{2,1,0:T(8,128)(2,1)}, u32[]{:S(2)}, u32[]{:S(2)}) async-start(bf16[64,6,2048]{2,1,0:T(8,128)(2,1)} %reshape.144), calls=%async_computation.1 | async-start | bytes 4194304 | tf_op jit(solution)/shard_map/all_to_all | solution.py:141
  164.3 3.6 %collective-permute-start = (bf16[15,1024]{1,0:T(8,128)(2,1)S(1)}, bf16[15,1024]{1,0:T(8,128)(2,1)S(1)}, u32[]{:S(2)}, u32[]{:S(2)}) collective-permute-start(bf16[15,1024]{1,0:T(8,128)(2,1)S(1)} %slice.93), channel_id=1, source_target_pairs={{0,1},{1,2},{2,3},{3,4},{4,5},{5,6},{6,7},{7,8},{8,9},{9,10},{10,1... | collective-permute-start | bytes 92168 | tf_op jit(solution)/shard_map/ppermute | solution.py:16
  168.5 45.4 %collective-permute-done = bf16[15,1024]{1,0:T(8,128)(2,1)S(1)} collective-permute-done((bf16[15,1024]{1,0:T(8,128)(2,1)S(1)}, bf16[15,1024]{1,0:T(8,128)(2,1)S(1)}, u32[]{:S(2)}, u32[]{:S(2)}) %collective-permute-start) | collective-permute-done | bytes 30752 | tf_op jit(solution)/shard_map/ppermute | solution.py:16
  214.2 1.9 fusion.18
  216.1 0.2 fusion.16
  216.3 2.2 convolution_convert_fusion.4
  218.6 2.6 %reshape.145 = bf16[384,2048]{1,0:T(8,128)(2,1)S(1)} reshape(bf16[64,6,2048]{2,1,0:T(8,128)(2,1)} %all-to-all-done.1) | data formatting | bytes 3145728 | tf_op jit(solution)/shard_map/reshape | solution.py:144
  221.2 1.4 gather_fusion.1
  222.6 1.3 reshape.147
  223.9 3.9 %multiply_reduce_fusion = bf16[128,2048]{1,0:T(8,128)(2,1)} fusion(f32[128,2,2048]{2,1,0:T(2,128)S(1)} %reshape.147, f32[128,2]{1,0:T(8,128)S(1)} %mul.78), kind=kLoop, calls=%fused_computation.14 | loop fusion | flops 786432 | bytes 2622464 | tf_op jit(solution)/shard_map/reduce_sum | solution.py:146
  (46 shorter events, 1.7 us)
Async XLA Ops:
  7.2 207.0 %copy-start = (bf16[8,128,128]{2,1,0:T(8,128)(2,1)S(1)}, bf16[8,128,128]{2,1,0:T(8,128)(2,1)}, u32[]{:S(2)}) copy-start(bf16[8,128,128]{2,1,0:T(8,128)(2,1)} %param.12) | copy-start | bytes 786436
  7.2 1.6 copy-start.1
  7.2 128.3 %all-gather.2.cloned.1.call-start = ((), (), s32[]{:S(2)}) async-start(), calls=%async_computation.2 | async-start | bytes 15728640 | tf_op jit(solution)/shard_map/all_gather | solution.py:22
  12.3 0.7 copy-start.5
  12.3 3.9 %copy-start.3 = (bf16[512,2048]{1,0:T(8,128)(2,1)S(1)}, bf16[512,2048]{1,0:T(8,128)(2,1)}, u32[]{:S(2)}) copy-start(bf16[512,2048]{1,0:T(8,128)(2,1)} %param.15) | copy-start | bytes 6291460
  12.4 4.1 %copy-start.4 = (f32[2048]{0:T(1024)S(1)}, f32[2048]{0:T(1024)}, u32[]{:S(2)}) copy-start(f32[2048]{0:T(1024)} %param.16) | copy-start | bytes 24580
  153.6 10.7 %copy-start.2 = (bf16[256,1024]{1,0:T(8,128)(2,1)S(1)}, bf16[256,1024]{1,0:T(8,128)(2,1)}, u32[]{:S(2)}) copy-start(bf16[256,1024]{1,0:T(8,128)(2,1)} %param.11) | copy-start | bytes 1572868
  153.6 14.4 %copy-start.6 = (f32[512,2]{0,1:T(2,128)S(1)}, f32[512,2]{0,1:T(2,128)}, u32[]{:S(2)}) copy-start(f32[512,2]{0,1:T(2,128)} %param.18) | copy-start | bytes 12292
  153.6 65.0 %all-to-all-start.1 = ((bf16[64,6,2048]{2,1,0:T(8,128)(2,1)}), bf16[64,6,2048]{2,1,0:T(8,128)(2,1)}, u32[]{:S(2)}, u32[]{:S(2)}) async-start(bf16[64,6,2048]{2,1,0:T(8,128)(2,1)} %reshape.144), calls=%async_computation.1 | async-start | bytes 4194304 | tf_op jit(solution)/shard_map/all_to_all | solution.py:141
  164.3 49.7 %collective-permute-start = (bf16[15,1024]{1,0:T(8,128)(2,1)S(1)}, bf16[15,1024]{1,0:T(8,128)(2,1)S(1)}, u32[]{:S(2)}, u32[]{:S(2)}) collective-permute-start(bf16[15,1024]{1,0:T(8,128)(2,1)S(1)} %slice.93), channel_id=1, source_target_pairs={{0,1},{1,2},{2,3},{3,4},{4,5},{5,6},{6,7},{7,8},{8,9},{9,10},{10,1... | collective-permute-start | bytes 92168 | tf_op jit(solution)/shard_map/ppermute | solution.py:16
  214.1 2.0 copy-start.7
  214.1 2.2 copy-start.8
Sparse Core Ops, SparseCore 0:
  12.5 122.9 all-gather.1
where the time goes:
time: 235 us
  waiting for transfers between devices  94.4 us (40%)
  blocking collectives  60 us (26%)
  local copies, waits for them, and re-layouts  20.7 us (9%)
  matrix products  19.5 us (8%)
  between operations  14.4 us (6%)
  starting transfers between devices  14.3 us (6%)
  other arithmetic  11.4 us (5%)
    all_to_all x1, blocking collectives, on_device(): lax.all_to_all(outgoing, 'ep', split_axis=1, concat_axis=1, tiled=True)  60 us
    all_gather x1, waiting for transfers between devices, rows_first(): out, at, gathered = (lax.all_gather(both, axis, axis=0, tiled=True), 0, [])  48.9 us
    ppermute x1, waiting for transfers between devices, passed_along(): return lax.ppermute(array, axis, pairs)  45.4 us
    all_to_all x1, starting transfers between devices, on_device(): lax.all_to_all(results, 'ep', split_axis=0, concat_axis=0, tiled=True)  10.6 us
    dot_general x4, matrix products, on_device(): jnp.dot(hidden[:, block * quarter:(block + 1) * quarter], down_whole[bloc...  7.21 us
  transfers between devices with their start and end apart: 3, of which 2 were waited for; matrix products, arithmetic and copies ran while one was open for 8% of the time, Pallas kernels for 0%

commit v1 on v0

--- a/solution.py
+++ b/solution.py
@@ -19,7 +19,13 @@
 def rows_first(arrays, axis, dims):
     turned = [jnp.moveaxis(a, dim, 0) for a, dim in zip(arrays, dims)]
     both = jnp.concatenate([t.reshape(len(t), -1) for t in turned], axis=1)
-    out, at, gathered = (lax.all_gather(both, axis, axis=0, tiled=True), 0, [])
+    out, at, gathered = (
+        jnp.concatenate(
+            lax.all_to_all(jnp.stack([both] * lax.axis_size(axis)), axis, 0, 0), axis=0
+        ),
+        0,
+        [],
+    )
     for t, dim in zip(turned, dims):
         piece = out[:, at : at + t[0].size].reshape(-1, *t.shape[1:])
         gathered.append(jnp.moveaxis(piece, 0, dim))

time: 235 us -> 314 us (1.34)
  waiting for transfers between devices: 94.4 us -> 225 us
  blocking collectives: 60 us -> 0 us
  starting transfers between devices: 14.3 us -> 28.9 us
  between operations: 14.4 us -> 1.03 us
  local copies, waits for them, and re-layouts: 20.7 us -> 26 us
    all_to_all x0 -> x2, waiting for transfers between devices: none -> 180 us  [the longest x1 135 us: rows_first(): lax.all_to_all(jnp.stack([both] * lax.axis_size(axis)), axis, 0, 0)]
    all_to_all x1 -> x0, blocking collectives: 60 us -> none  [on_device(): lax.all_to_all(outgoing, 'ep', split_axis=1, concat_axis=1, tiled=True)]
    all_gather x1 -> x0, waiting for transfers between devices: 48.9 us -> none  [rows_first(): out, at, gathered = (lax.all_gather(both, axis, axis=0, tiled=True), 0, [])]
    all_to_all x0 -> x2, starting transfers between devices: none -> 17.6 us  [the longest x1 11 us: on_device(): lax.all_to_all(outgoing, 'ep', split_axis=1, concat_axis=1, tiled=True)]
    another operation x2 -> x3, local copies, waits for them, and re-layouts: 0.01 us -> 6.05 us  [the longest x1 6.04 us: rows_first(): jnp.stack([both] * lax.axis_size(axis))]
  transfers between devices with their start and end apart: 3 -> 4, of which waited for: 2 -> 3; matrix products, arithmetic and copies ran while one was open for 8% -> 4% of each run, Pallas kernels for 0% -> 0%
where the time goes in v1:
time: 314 us; the launch traced here: 313 us
  waiting for transfers between devices  225 us (72%)
  starting transfers between devices  28.9 us (9%)
  local copies, waits for them, and re-layouts  26 us (8%)
  matrix products  19.5 us (6%)
  other arithmetic  12.6 us (4%)
    all_to_all x1, waiting for transfers between devices, rows_first(): lax.all_to_all(jnp.stack([both] * lax.axis_size(axis)), axis, 0, 0)  135 us
    ppermute x1, waiting for transfers between devices, passed_along(): return lax.ppermute(array, axis, pairs)  45.6 us
    all_to_all x1, waiting for transfers between devices, on_device(): lax.all_to_all(outgoing, 'ep', split_axis=1, concat_axis=1, tiled=True)  44.4 us
    all_to_all x1, starting transfers between devices, on_device(): lax.all_to_all(outgoing, 'ep', split_axis=1, concat_axis=1, tiled=True)  11 us
    all_to_all x1, starting transfers between devices, on_device(): lax.all_to_all(results, 'ep', split_axis=0, concat_axis=0, tiled=True)  8.56 us
    dot_general x4, matrix products, on_device(): jnp.dot(hidden[:, block * quarter:(block + 1) * quarter], down_whole[bloc...  7.21 us
    all_to_all x1, starting transfers between devices, rows_first(): lax.all_to_all(jnp.stack([both] * lax.axis_size(axis)), axis, 0, 0)  6.51 us
  transfers between devices with their start and end apart: 4, of which 3 were waited for; matrix products, arithmetic and copies ran while one was open for 4% of the time, Pallas kernels for 0%

profile of v1, /device:TPU:96, one launch (start us, length us, event | category | flops | bytes accessed | tf_op | source)
XLA Modules:
  0.0 313.3 jit_solution(11947091503206739326)
XLA Ops:
  1.9 1.2 fusion.6
  3.2 2.4 reduce-window.6
  6.0 1.4 scatter_custom_fusion
  7.5 1.2 fusion.8
  8.8 2.5 gather_fusion
  11.2 1.6 broadcast_in_dim_reshape.4
  12.9 11.0 %all-to-all-start = ((bf16[1,64,6,2048]{3,2,0,1:T(8,128)(2,1)}), bf16[1,64,6,2048]{3,2,0,1:T(8,128)(2,1)}, u32[]{:S(2)}, u32[]{:S(2)}) async-start(bf16[1,64,6,2048]{3,2,0,1:T(8,128)(2,1)} %bitcast.6), calls=%async_computation | async-start | bytes 4194304 | tf_op jit(solution)/shard_map/all_to_all | solution.py:131
  24.0 1.4 copy.36
  25.4 1.4 copy.35
  26.8 2.0 pad_maximum_fusion
  28.8 44.4 %all-to-all-done = bf16[1,64,6,2048]{3,2,0,1:T(8,128)(2,1)} async-done(((bf16[1,64,6,2048]{3,2,0,1:T(8,128)(2,1)}), bf16[1,64,6,2048]{3,2,0,1:T(8,128)(2,1)}, u32[]{:S(2)}, u32[]{:S(2)}) %all-to-all-start) | async-done | bytes 1572896 | tf_op jit(solution)/shard_map/all_to_all | solution.py:131
  73.3 6.0 %stack.2 = bf16[4,256,6144]{2,1,0:T(8,128)(2,1)} broadcast(bf16[256,6144]{1,0:T(8,128)(2,1)S(1)} %pad_maximum_fusion), dimensions={1,2} | broadcast | bytes 15728640 | tf_op jit(solution)/shard_map/stack | solution.py:24
  79.3 6.5 %all-to-all-start.1 = ((bf16[4,256,6144]{2,1,0:T(8,128)(2,1)}), bf16[4,256,6144]{2,1,0:T(8,128)(2,1)}, u32[]{:S(2)}, u32[]{:S(2)}) async-start(bf16[4,256,6144]{2,1,0:T(8,128)(2,1)} %stack.2), calls=%async_computation.1 | async-start | bytes 25165824 | tf_op jit(solution)/shard_map/all_to_all | solution.py:24
  85.8 2.6 reshape.148
  88.4 135.3 %all-to-all-done.1 = bf16[4,256,6144]{2,1,0:T(8,128)(2,1)} async-done(((bf16[4,256,6144]{2,1,0:T(8,128)(2,1)}), bf16[4,256,6144]{2,1,0:T(8,128)(2,1)}, u32[]{:S(2)}, u32[]{:S(2)}) %all-to-all-start.1) | async-done | bytes 12582944 | tf_op jit(solution)/shard_map/all_to_all | solution.py:24
  223.7 4.0 %fusion.2 = f32[384,1024]{1,0:T(8,128)S(1)} fusion(bf16[384,2048]{1,0:T(8,128)(2,1)S(1)} %reshape.148, bf16[1024,6144]{1,0:T(8,128)(2,1)} %bitcast.12), kind=kOutput, calls=%fused_computation.5 | convolution fusion | flops 1610612736 | bytes 7340032 | tf_op jit(solution)/shard_map/dot_general | solution.py:133
  227.7 4.1 %multiply_convert_fusion = bf16[384,1024]{1,0:T(8,128)(2,1)S(1)} fusion(f32[384,1024]{1,0:T(8,128)S(1)} %fusion.2, bf16[384,2048]{1,0:T(8,128)(2,1)S(1)} %reshape.148, bf16[1024,6144]{1,0:T(8,128)(2,1)} %bitcast.12), kind=kOutput, calls=%fused_computation.15 | convolution fusion | flops 1612972032 | bytes 8126464 | tf_op jit(solution)/shard_map/dot_general | solution.py:134
  231.9 1.8 convolution_convert_fusion
  233.7 1.8 convolution_convert_fusion.1
  235.5 1.8 convolution_convert_fusion.2
  237.3 1.8 convolution_convert_fusion.3
  239.1 1.2 add_convert_fusion
  240.3 1.6 reshape.150
  241.9 8.6 %all-to-all-start.2 = ((bf16[64,6,2048]{2,1,0:T(8,128)(2,1)}), bf16[64,6,2048]{2,1,0:T(8,128)(2,1)}, u32[]{:S(2)}, u32[]{:S(2)}) async-start(bf16[64,6,2048]{2,1,0:T(8,128)(2,1)} %reshape.150), calls=%async_computation.2 | async-start | bytes 4194304 | tf_op jit(solution)/shard_map/all_to_all | solution.py:147
  250.5 2.7 collective-permute-start
  253.8 45.6 %collective-permute-done = bf16[15,1024]{1,0:T(8,128)(2,1)S(1)} collective-permute-done((bf16[15,1024]{1,0:T(8,128)(2,1)S(1)}, bf16[15,1024]{1,0:T(8,128)(2,1)S(1)}, u32[]{:S(2)}, u32[]{:S(2)}) %collective-permute-start) | collective-permute-done | bytes 30752 | tf_op jit(solution)/shard_map/ppermute | solution.py:16
  299.6 1.9 fusion.18
  301.8 2.2 convolution_convert_fusion.4
  304.1 2.6 reshape.151
  306.7 1.4 gather_fusion.1
  308.1 1.3 reshape.153
  309.4 3.9 %multiply_reduce_fusion = bf16[128,2048]{1,0:T(8,128)(2,1)} fusion(f32[128,2,2048]{2,1,0:T(2,128)S(1)} %reshape.153, f32[128,2]{1,0:T(8,128)S(1)} %mul.78), kind=kLoop, calls=%fused_computation.14 | loop fusion | flops 786432 | bytes 2622464 | tf_op jit(solution)/shard_map/reduce_sum | solution.py:152
  (45 shorter events, 2.7 us)
Async XLA Ops:
  0.6 299.0 %copy-start = (bf16[8,128,128]{2,1,0:T(8,128)(2,1)S(1)}, bf16[8,128,128]{2,1,0:T(8,128)(2,1)}, u32[]{:S(2)}) copy-start(bf16[8,128,128]{2,1,0:T(8,128)(2,1)} %param.12) | copy-start | bytes 786436
  0.6 6.8 %copy-start.4 = (f32[2048]{0:T(1024)S(1)}, f32[2048]{0:T(1024)}, u32[]{:S(2)}) copy-start(f32[2048]{0:T(1024)} %param.16) | copy-start | bytes 24580
  12.9 11.1 %copy-start.1 = (bf16[1,2048,256]{2,1,0:T(8,128)(2,1)S(1)}, bf16[1,2048,256]{2,1,0:T(8,128)(2,1)}, u32[]{:S(2)}) copy-start(bf16[1,2048,256]{2,1,0:T(8,128)(2,1)} %param.20) | copy-start | bytes 3145732
  12.9 60.4 %all-to-all-start = ((bf16[1,64,6,2048]{3,2,0,1:T(8,128)(2,1)}), bf16[1,64,6,2048]{3,2,0,1:T(8,128)(2,1)}, u32[]{:S(2)}, u32[]{:S(2)}) async-start(bf16[1,64,6,2048]{3,2,0,1:T(8,128)(2,1)} %bitcast.6), calls=%async_computation | async-start | bytes 4194304 | tf_op jit(solution)/shard_map/all_to_all | solution.py:131
  23.9 1.4 copy-start.2
  79.3 144.4 %all-to-all-start.1 = ((bf16[4,256,6144]{2,1,0:T(8,128)(2,1)}), bf16[4,256,6144]{2,1,0:T(8,128)(2,1)}, u32[]{:S(2)}, u32[]{:S(2)}) async-start(bf16[4,256,6144]{2,1,0:T(8,128)(2,1)} %stack.2), calls=%async_computation.1 | async-start | bytes 25165824 | tf_op jit(solution)/shard_map/all_to_all | solution.py:24
  241.9 8.6 %copy-start.3 = (bf16[256,1024]{1,0:T(8,128)(2,1)S(1)}, bf16[256,1024]{1,0:T(8,128)(2,1)}, u32[]{:S(2)}) copy-start(bf16[256,1024]{1,0:T(8,128)(2,1)} %param.11) | copy-start | bytes 1572868
  241.9 11.4 %copy-start.5 = (f32[512,2]{0,1:T(2,128)S(1)}, f32[512,2]{0,1:T(2,128)}, u32[]{:S(2)}) copy-start(f32[512,2]{0,1:T(2,128)} %param.18) | copy-start | bytes 12292
  241.9 62.2 %all-to-all-start.2 = ((bf16[64,6,2048]{2,1,0:T(8,128)(2,1)}), bf16[64,6,2048]{2,1,0:T(8,128)(2,1)}, u32[]{:S(2)}, u32[]{:S(2)}) async-start(bf16[64,6,2048]{2,1,0:T(8,128)(2,1)} %reshape.150), calls=%async_computation.2 | async-start | bytes 4194304 | tf_op jit(solution)/shard_map/all_to_all | solution.py:147
  250.5 49.0 %collective-permute-start = (bf16[15,1024]{1,0:T(8,128)(2,1)S(1)}, bf16[15,1024]{1,0:T(8,128)(2,1)S(1)}, u32[]{:S(2)}, u32[]{:S(2)}) collective-permute-start(bf16[15,1024]{1,0:T(8,128)(2,1)S(1)} %slice.93), channel_id=1, source_target_pairs={{0,1},{1,2},{2,3},{3,4},{4,5},{5,6},{6,7},{7,8},{8,9},{9,10},{10,1... | collective-permute-start | bytes 92168 | tf_op jit(solution)/shard_map/ppermute | solution.py:16
  299.6 2.0 copy-start.6
  299.6 2.2 copy-start.7
